TPU v7x, 256 devices: a whole 4x4x8 slice. The times are simulated.
256 devices in a mesh: ra: 32 (over z, y), cb: 4 (over x), dp: 2 (over core).
Axes of the slice: x: 4, y: 4, z: 8, core: 2. Of those that a mesh axis runs over, the one named last changes fastest.
Arguments:
- stream: bfloat16 [3072, 4096], P(('cb', 'dp'), 'ra'), may hold values from -20 to 20
- up_first: bfloat16 [4096, 16384], P('cb', 'ra'), may hold values from -0.09375 to 0.09375
- down_first: bfloat16 [16384, 4096], P('ra', 'cb'), may hold values from -0.046875 to 0.046875
- up_second: bfloat16 [4096, 16384], P('cb', 'ra'), may hold values from -0.09375 to 0.09375
- down_second: bfloat16 [16384, 4096], P('ra', 'cb'), may hold values from -0.046875 to 0.046875
- gain_first: float32 [4096], P('ra'), may hold values from 0.1 to 1.9
- bias_first: float32 [4096], P('ra'), may hold values from -3 to 3
- gain_second: float32 [4096], P('ra'), may hold values from 0.1 to 1.9
- bias_second: float32 [4096], P('ra'), may hold values from -3 to 3
Outputs:
- result: bfloat16 [3072, 4096], P(('cb', 'dp'), 'ra')
All inputs are finite; a program needn't handle non-finite values.
Results may differ from a plain program's by a relative error of at most 0.0093.
Values may be sent and summed in bfloat16 or wider, within the bound.
No kernel may reach another device: no remote copies, remote signals or barrier semaphores. Data moves between devices by JAX's collectives and lax.ppermute only.
A program may use at most 64 MiB of HBM per device.

v0:
```python
import jax
import jax.numpy as jnp
from jax import lax
from jax.sharding import Mesh
from jax.sharding import PartitionSpec as P

RA = ("ra_0", "ra_1")
RESID = 1.4142135
EPS = 0.5


def whole_of(shard, axes, dim):
    for axis in reversed(axes):
        shard = lax.all_gather(shard, axis, axis=dim, tiled=True)
    return shard


def cut_along(shard, dim, length):
    lengths = shard.shape
    blocks = shard.reshape(*lengths[:dim], length, lengths[dim] // length, *lengths[dim + 1 :])
    return jnp.moveaxis(blocks, dim, 0)


def summed_on_arrival(shard, axis, dim):
    length = lax.axis_size(axis)
    blocks = lax.all_to_all(cut_along(shard, dim, length), axis, 0, 0, tiled=True)
    return jnp.sum(blocks.astype(jnp.float32), axis=0)


def copy_for_each(shard, axis):
    length = lax.axis_size(axis)
    return lax.all_to_all(
        jnp.broadcast_to(shard[None], (length, *shard.shape)), axis, 0, 0, tiled=True
    )


def over_copies(shard, axis):
    everything = copy_for_each(shard, axis)
    return jnp.sum(everything, axis=0)


def in_one(arrays, axis):
    ravelled, at, done = (jnp.concatenate([a.reshape(-1) for a in arrays]), 0, [])
    subtotal = over_copies(ravelled, axis)
    for a in arrays:
        done.append(subtotal[at : at + a.size].reshape(a.shape))
        at += a.size
    return tuple(done)


def sublayer(x, up, down, gain, bias):
    whole = whole_of(x, RA, 1)
    pre = jnp.dot(
        whole, lax.all_gather(up, "cb", axis=0, tiled=True), preferred_element_type=jnp.float32
    )
    hidden = jnp.square(jax.nn.relu(pre)).astype(jnp.bfloat16)
    partial_sums = jnp.dot(
        hidden, lax.all_gather(down, "cb", axis=1, tiled=True), preferred_element_type=jnp.float32
    )
    branch = summed_on_arrival(partial_sums.astype(jnp.bfloat16), RA, 1)
    mixed = RESID * x.astype(jnp.float32) + branch
    width = mixed.shape[1] * lax.axis_size(RA)
    total, squares = in_one(
        (jnp.sum(mixed, axis=1, keepdims=True), jnp.sum(mixed * mixed, axis=1, keepdims=True)), RA
    )
    mean = total / width
    var = squares / width - mean * mean
    centered = mixed - mean
    return (centered * lax.rsqrt(var + EPS) * gain + bias).astype(jnp.bfloat16)


def body(
    stream,
    up_first,
    down_first,
    up_second,
    down_second,
    gain_first,
    bias_first,
    gain_second,
    bias_second,
):
    x = stream
    for up, down, gain, bias in (
        (up_first, down_first, gain_first, bias_first),
        (up_second, down_second, gain_second, bias_second),
    ):
        x = sublayer(x, up, down, gain, bias)
    return x


def solution(mesh):
    torus = Mesh(
        mesh.devices.reshape(8, 4, mesh.shape["cb"], mesh.shape["dp"]), ("ra_0", "ra_1", "cb", "dp")
    )
    in_specs = (
        P(("cb", "dp"), RA),
        P("cb", RA),
        P(RA, "cb"),
        P("cb", RA),
        P(RA, "cb"),
        P(RA),
        P(RA),
        P(RA),
        P(RA),
    )
    out_specs = P(("cb", "dp"), RA)
    return jax.shard_map(body, mesh=torus, in_specs=in_specs, out_specs=out_specs, check_vma=False)
```

profile of v0, /device:TPU:2, one launch (start us, length us, event | category | flops | bytes accessed | tf_op | source)
XLA Modules:
  0.0 448.1 jit_solution(4265126801284976559)
XLA Ops:
  6.5 0.0 all-gather.7.cloned.1.call-start
  6.5 13.8 %all_gather.24 = bf16[384,512]{1,0:T(8,128)(2,1)} all-gather(bf16[384,128]{1,0:T(8,128)(2,1)} %param.9), channel_id=1, replica_groups=mesh['ra_0'=8,'ra_1'=4,'cb'=4,'dp'=2] {'ra_1'}, dimensions={1}, use_global_device_ids=true | all-gather | bytes 491520 | tf_op jit(solution)/shard_map/all_gather | solution.py:14
  20.4 0.0 all-gather.7.cloned.1.call-update
  20.4 0.0 all-gather.11.cloned.1.call-start
  20.5 0.7 all-gather.11.cloned.1.call-update
  21.2 0.0 all-gather.9.cloned.1.call-start
  21.2 0.7 all-gather.9.cloned.1.call-update
  21.9 0.0 all-gather.15.cloned.1.call-start
  21.9 0.5 all-gather.15.cloned.1.call-update
  22.5 46.4 %all-gather.7.cloned.1.call-done = bf16[384,4096]{1,0:T(8,128)(2,1)} async-done(((bf16[384,512]{1,0:T(8,128)(2,1)}), bf16[384,4096]{1,0:T(8,128)(2,1)}) %all-gather.7.cloned.1.call-update) | async-done | bytes 3145744 | tf_op jit(solution)/shard_map/all_gather | solution.py:14
  68.9 50.6 %all-gather.11.cloned.1.call-done = bf16[512,4096]{1,0:T(8,128)(2,1)} async-done(((bf16[512,1024]{1,0:T(8,128)(2,1)}), bf16[512,4096]{1,0:T(8,128)(2,1)}) %all-gather.11.cloned.1.call-update) | async-done | bytes 4194320 | tf_op jit(solution)/shard_map/all_gather | solution.py:58
  119.4 53.0 %all-gather.9.cloned.1.call-done = bf16[4096,512]{1,0:T(8,128)(2,1)} async-done(((bf16[1024,512]{1,0:T(8,128)(2,1)}), bf16[4096,512]{1,0:T(8,128)(2,1)}) %all-gather.9.cloned.1.call-update) | async-done | bytes 4194320 | tf_op jit(solution)/shard_map/all_gather | solution.py:54
  172.4 7.8 %fusion = bf16[48,32,8,128]{3,2,1,0:T(8,128)(2,1)S(1)} fusion(bf16[512,4096]{1,0:T(8,128)(2,1)} %all-gather.11.cloned.1.call-done, bf16[384,4096]{1,0:T(8,128)(2,1)} %all-gather.7.cloned.1.call-done, bf16[4096,512]{1,0:T(8,128)(2,1)} %all-gather.9.cloned.1.call-done), kind=kOutput, calls=%fused_computation.6 | convolution fusion | flops 3223388160 | bytes 14680064 | tf_op jit(solution)/shard_map/dot_general | solution.py:57
  180.2 2.6 copy.29
  182.8 0.0 copy-start
  182.8 0.0 copy-start.1
  182.8 10.0 %all-to-all-start = ((bf16[32,384,128]{2,1,0:T(8,128)(2,1)}), bf16[32,384,128]{2,1,0:T(8,128)(2,1)S(1)}, u32[]{:S(2)}, u32[]{:S(2)}) async-start(bf16[32,384,128]{2,1,0:T(8,128)(2,1)} %bitcast.22), calls=%async_computation | async-start | bytes 6291456 | tf_op jit(solution)/shard_map/all_to_all | solution.py:26
  192.8 0.0 all-gather.17.cloned.1.call-start
  192.9 0.5 all-gather.17.cloned.1.call-update
  193.4 0.0 all-gather.13.cloned.1.call-start
  193.5 71.5 %all-to-all-done = bf16[32,384,128]{2,1,0:T(8,128)(2,1)S(1)} async-done(((bf16[32,384,128]{2,1,0:T(8,128)(2,1)}), bf16[32,384,128]{2,1,0:T(8,128)(2,1)S(1)}, u32[]{:S(2)}, u32[]{:S(2)}) %all-to-all-start) | async-done | bytes 3145760 | tf_op jit(solution)/shard_map/all_to_all | solution.py:26
  264.9 0.4 convert_reduce_fusion.1
  265.4 0.0 copy-done
  265.4 0.2 fusion.8
  265.6 0.1 broadcast_in_dim.4
  265.6 16.4 %all_to_all.22 = f32[32,1,768]{2,1,0:T(1,128)S(1)} all-to-all(f32[32,1,768]{2,1,0:T(1,128)S(1)} %broadcast_in_dim.4), channel_id=1, replica_groups=mesh['ra_0'=8,'ra_1'=4,'cb'=4,'dp'=2] {'ra_0','ra_1'}, dimensions={0} | all-to-all | bytes 196608 | tf_op jit(solution)/shard_map/all_to_all | solution.py:32
  282.0 0.1 reduce_sum.75
  282.1 0.0 copy-done.1
  282.1 0.0 copy-done.2
  282.1 0.2 add_convert_fusion.1
  282.3 12.7 %all_gather.28 = bf16[384,512]{1,0:T(8,128)(2,1)} all-gather(bf16[384,128]{1,0:T(8,128)(2,1)S(1)} %add_convert_fusion.1), channel_id=1, replica_groups=mesh['ra_0'=8,'ra_1'=4,'cb'=4,'dp'=2] {'ra_1'}, dimensions={1}, use_global_device_ids=true | all-gather | bytes 491520 | tf_op jit(solution)/shard_map/all_gather | solution.py:14
  295.0 0.0 all-gather.13.cloned.1.call-update
  295.0 0.0 all-gather.15.cloned.1.call-done
  295.0 0.0 all-gather.17.cloned.1.call-done
  295.1 40.6 %all-gather.13.cloned.1.call-done = bf16[384,4096]{1,0:T(8,128)(2,1)} async-done(((bf16[384,512]{1,0:T(8,128)(2,1)}), bf16[384,4096]{1,0:T(8,128)(2,1)}) %all-gather.13.cloned.1.call-update) | async-done | bytes 3145744 | tf_op jit(solution)/shard_map/all_gather | solution.py:14
  335.7 7.8 %fusion.1 = bf16[48,32,8,128]{3,2,1,0:T(8,128)(2,1)S(1)} fusion(bf16[512,4096]{1,0:T(8,128)(2,1)} %all-gather.17.cloned.1.call-done, bf16[384,4096]{1,0:T(8,128)(2,1)} %all-gather.13.cloned.1.call-done, bf16[4096,512]{1,0:T(8,128)(2,1)} %all-gather.15.cloned.1.call-done), kind=kOutput, calls=%fused_computation.7 | convolution fusion | flops 3223388160 | bytes 14680064 | tf_op jit(solution)/shard_map/dot_general | solution.py:57
  343.5 0.9 copy.28
  344.4 0.0 copy-start.3
  344.4 0.0 copy-start.4
  344.4 79.6 %all_to_all.23 = bf16[32,384,128]{2,1,0:T(8,128)(2,1)S(1)} all-to-all(bf16[32,384,128]{2,1,0:T(8,128)(2,1)S(1)} %bitcast.23), channel_id=1, replica_groups=mesh['ra_0'=8,'ra_1'=4,'cb'=4,'dp'=2] {'ra_0','ra_1'}, dimensions={0} | all-to-all | bytes 6291456 | tf_op jit(solution)/shard_map/all_to_all | solution.py:26
  424.1 0.4 convert_reduce_fusion
  424.5 0.2 fusion.9
  424.7 0.1 broadcast_in_dim.5
  424.8 15.6 %all_to_all.24 = f32[32,1,768]{2,1,0:T(1,128)S(1)} all-to-all(f32[32,1,768]{2,1,0:T(1,128)S(1)} %broadcast_in_dim.5), channel_id=1, replica_groups=mesh['ra_0'=8,'ra_1'=4,'cb'=4,'dp'=2] {'ra_0','ra_1'}, dimensions={0} | all-to-all | bytes 196608 | tf_op jit(solution)/shard_map/all_to_all | solution.py:32
  440.4 0.1 reduce_sum.79
  440.5 0.0 copy-done.3
  440.5 0.0 copy-done.4
  440.5 0.8 add_convert_fusion
  (5 shorter events, 0.0 us)
Async XLA Ops:
  6.5 62.3 %all-gather.7.cloned.1.call-start = ((), (), s32[]{:S(2)}) async-start(), calls=%async_computation.4 | async-start | bytes 3538944 | tf_op jit(solution)/shard_map/all_gather | solution.py:14
  20.4 99.0 %all-gather.11.cloned.1.call-start = ((), (), s32[]{:S(2)}) async-start(), calls=%async_computation.6 | async-start | bytes 5242880 | tf_op jit(solution)/shard_map/all_gather | solution.py:58
  21.2 151.2 %all-gather.9.cloned.1.call-start = ((), (), s32[]{:S(2)}) async-start(), calls=%async_computation.5 | async-start | bytes 5242880 | tf_op jit(solution)/shard_map/all_gather | solution.py:54
  21.9 273.1 %all-gather.15.cloned.1.call-start = ((), (), s32[]{:S(2)}) async-start(), calls=%async_computation.8 | async-start | bytes 5242880 | tf_op jit(solution)/shard_map/all_gather | solution.py:54
  182.8 82.5 %copy-start = (bf16[384,128]{1,0:T(8,128)(2,1)S(1)}, bf16[384,128]{1,0:T(8,128)(2,1)}, u32[]{:S(2)}) copy-start(bf16[384,128]{1,0:T(8,128)(2,1)} %param.9) | copy-start | bytes 294916
  182.8 99.3 %copy-start.1 = (f32[128]{0:T(128)S(1)}, f32[128]{0:T(128)}, u32[]{:S(2)}) copy-start(f32[128]{0:T(128)} %param.15) | copy-start | bytes 1540
  182.8 99.3 %copy-start.2 = (f32[128]{0:T(128)S(1)}, f32[128]{0:T(128)}, u32[]{:S(2)}) copy-start(f32[128]{0:T(128)} %param.14) | copy-start | bytes 1540
  182.8 82.1 %all-to-all-start = ((bf16[32,384,128]{2,1,0:T(8,128)(2,1)}), bf16[32,384,128]{2,1,0:T(8,128)(2,1)S(1)}, u32[]{:S(2)}, u32[]{:S(2)}) async-start(bf16[32,384,128]{2,1,0:T(8,128)(2,1)} %bitcast.22), calls=%async_computation | async-start | bytes 6291456 | tf_op jit(solution)/shard_map/all_to_all | solution.py:26
  192.8 102.2 %all-gather.17.cloned.1.call-start = ((), (), s32[]{:S(2)}) async-start(), calls=%async_computation.9 | async-start | bytes 5242880 | tf_op jit(solution)/shard_map/all_gather | solution.py:58
  193.4 142.3 %all-gather.13.cloned.1.call-start = ((), (), s32[]{:S(2)}) async-start(), calls=%async_computation.7 | async-start | bytes 3538944 | tf_op jit(solution)/shard_map/all_gather | solution.py:14
  344.4 96.0 %copy-start.3 = (f32[128]{0:T(128)S(1)}, f32[128]{0:T(128)}, u32[]{:S(2)}) copy-start(f32[128]{0:T(128)} %param.17) | copy-start | bytes 1540
  344.4 96.0 %copy-start.4 = (f32[128]{0:T(128)S(1)}, f32[128]{0:T(128)}, u32[]{:S(2)}) copy-start(f32[128]{0:T(128)} %param.16) | copy-start | bytes 1540
Sparse Core Ops, SparseCore 0:
  20.5 48.2 all-gather.6
  70.7 48.7 all-gather.10
  121.2 51.0 all-gather.8
  174.0 51.0 all-gather.14
  226.8 51.0 all-gather.16
  295.1 40.5 all-gather.12
where the time goes:
time: 448 us
  waiting for transfers between devices  265 us (59%)
  blocking collectives  138 us (31%)
  matrix products  15.7 us (4%)
  between operations  13.6 us (3%)
  starting transfers between devices  10.2 us (2%)
    all_gather x2, waiting for transfers between devices, whole_of(): shard = lax.all_gather(shard, axis, axis=dim, tiled=True)  87 us
    all_to_all x1, blocking collectives, summed_on_arrival(): lax.all_to_all(cut_along(shard, dim, length), axis, 0, 0, tiled=True)  79.6 us
    all_to_all x1, waiting for transfers between devices, summed_on_arrival(): lax.all_to_all(cut_along(shard, dim, length), axis, 0, 0, tiled=True)  71.5 us
    all_gather x2, waiting for transfers between devices, sublayer(): lax.all_gather(up, 'cb', axis=0, tiled=True)  53 us
    all_gather x2, waiting for transfers between devices, sublayer(): lax.all_gather(down, 'cb', axis=1, tiled=True)  50.6 us
    all_to_all x2, blocking collectives, copy_for_each(): lax.all_to_all(jnp.broadcast_to(shard[None], (length, *shard.shape)), axi...  31.9 us
    all_gather x2, blocking collectives, whole_of(): shard = lax.all_gather(shard, axis, axis=dim, tiled=True)  26.5 us
    dot_general x2, matrix products, sublayer(): jnp.dot(hidden, lax.all_gather(down, 'cb', axis=1, tiled=True), preferred...  15.7 us
  transfers between devices with their start and end apart: 7, of which 5 were waited for; matrix products, arithmetic and copies ran while one was open for 3% of the time, Pallas kernels for 0%

commit v1 on v0

--- a/solution.py
+++ b/solution.py
@@ -7,6 +7,14 @@
 RA = ("ra_0", "ra_1")
 RESID = 1.4142135
 EPS = 0.5
+
+
+def tiled_gather(shard, axis, dim):
+    size = lax.axis_size(axis)
+    repeats = [size if d == dim else 1 for d in range(shard.ndim)]
+    return lax.all_to_all(
+        jnp.tile(shard, repeats), axis, split_axis=dim, concat_axis=dim, tiled=True
+    )
 
 
 def whole_of(shard, axes, dim):
@@ -54,9 +62,7 @@
         whole, lax.all_gather(up, "cb", axis=0, tiled=True), preferred_element_type=jnp.float32
     )
     hidden = jnp.square(jax.nn.relu(pre)).astype(jnp.bfloat16)
-    partial_sums = jnp.dot(
-        hidden, lax.all_gather(down, "cb", axis=1, tiled=True), preferred_element_type=jnp.float32
-    )
+    partial_sums = jnp.dot(hidden, tiled_gather(down, "cb", 1), preferred_element_type=jnp.float32)
     branch = summed_on_arrival(partial_sums.astype(jnp.bfloat16), RA, 1)
     mixed = RESID * x.astype(jnp.float32) + branch
     width = mixed.shape[1] * lax.axis_size(RA)

time: 448 us -> 406 us (0.906)
  waiting for transfers between devices: 265 us -> 112 us
  blocking collectives: 138 us -> 232 us
  local copies, waits for them, and re-layouts: 3.6 us -> 19.4 us
    all_to_all x0 -> x2, blocking collectives: none -> 98.2 us  [tiled_gather(): lax.all_to_all(jnp.tile(shard, repeats), axis, split_axis=dim, concat_axi...]
    all_gather x2, waiting for transfers between devices: 87 us -> 0.01 us  [whole_of(): shard = lax.all_gather(shard, axis, axis=dim, tiled=True)]
    all_gather x2 -> x0, waiting for transfers between devices: 50.6 us -> none  [sublayer(): lax.all_gather(down, 'cb', axis=1, tiled=True)]
    all_gather x2, waiting for transfers between devices: 53 us -> 39.7 us  [sublayer(): lax.all_gather(up, 'cb', axis=0, tiled=True)]
    all_to_all x0 -> x2, local copies, waits for them, and re-layouts: none -> 12.4 us  [tiled_gather(): lax.all_to_all(jnp.tile(shard, repeats), axis, split_axis=dim, concat_axi...]
    all_to_all x1, blocking collectives: 79.6 us -> 74.9 us  [summed_on_arrival(): lax.all_to_all(cut_along(shard, dim, length), axis, 0, 0, tiled=True)]
  transfers between devices with their start and end apart: 7 -> 5, of which waited for: 5 -> 2; matrix products, arithmetic and copies ran while one was open for 3% -> 4% of each run, Pallas kernels for 0% -> 0%
where the time goes in v1:
time: 406 us; the launch traced here: 405 us
  blocking collectives  232 us (57%)
  waiting for transfers between devices  112 us (28%)
  local copies, waits for them, and re-layouts  19.4 us (5%)
  matrix products  15.6 us (4%)
  between operations  13.3 us (3%)
  starting transfers between devices  10.1 us (2%)
    all_to_all x2, blocking collectives, tiled_gather(): lax.all_to_all(jnp.tile(shard, repeats), axis, split_axis=dim, concat_axi...  98.2 us
    all_to_all x1, blocking collectives, summed_on_arrival(): lax.all_to_all(cut_along(shard, dim, length), axis, 0, 0, tiled=True)  74.9 us
    all_to_all x1, waiting for transfers between devices, summed_on_arrival(): lax.all_to_all(cut_along(shard, dim, length), axis, 0, 0, tiled=True)  71.3 us
    all_gather x2, waiting for transfers between devices, sublayer(): lax.all_gather(up, 'cb', axis=0, tiled=True)  39.7 us
    all_to_all x2, blocking collectives, copy_for_each(): lax.all_to_all(jnp.broadcast_to(shard[None], (length, *shard.shape)), axi...  31.9 us
    all_gather x2, blocking collectives, whole_of(): shard = lax.all_gather(shard, axis, axis=dim, tiled=True)  26.5 us
    dot_general x2, matrix products, sublayer(): jnp.dot(hidden, tiled_gather(down, 'cb', 1), preferred_element_type=jnp.f...  15.6 us
    all_to_all x2, local copies, waits for them, and re-layouts, tiled_gather(): lax.all_to_all(jnp.tile(shard, repeats), axis, split_axis=dim, concat_axi...  12.4 us
  transfers between devices with their start and end apart: 5, of which 2 were waited for; matrix products, arithmetic and copies ran while one was open for 4% of the time, Pallas kernels for 0%

profile of v1, /device:TPU:2, one launch (start us, length us, event | category | flops | bytes accessed | tf_op | source)
XLA Modules:
  0.0 404.8 jit_solution(9513310780894151448)
XLA Ops:
  6.5 0.0 all-gather.5.cloned.1.call-start
  6.5 13.8 %all_gather.18 = bf16[384,512]{1,0:T(8,128)(2,1)} all-gather(bf16[384,128]{1,0:T(8,128)(2,1)} %param.9), channel_id=1, replica_groups=mesh['ra_0'=8,'ra_1'=4,'cb'=4,'dp'=2] {'ra_1'}, dimensions={1}, use_global_device_ids=true | all-gather | bytes 491520 | tf_op jit(solution)/shard_map/all_gather | solution.py:22
  20.4 0.0 all-gather.5.cloned.1.call-update
  20.4 0.0 all-gather.7.cloned.1.call-start
  20.4 0.7 all-gather.7.cloned.1.call-update
  21.1 1.7 tile.4
  22.9 50.6 %all_to_all.40 = bf16[512,4,1024]{2,0,1:T(8,128)(2,1)} all-to-all(bf16[512,4,1024]{2,0,1:T(8,128)(2,1)S(1)} %tile.4), channel_id=1, replica_groups=mesh['ra_0'=8,'ra_1'=4,'cb'=4,'dp'=2] {'cb'}, dimensions={1} | all-to-all | bytes 8388608 | tf_op jit(solution)/shard_map/all_to_all | solution.py:15
  73.5 6.2 %copy.20 = bf16[512,4,1024]{0,2,1:T(8,128)(2,1)} copy(bf16[512,4,1024]{2,0,1:T(8,128)(2,1)} %all_to_all.40) | data formatting | bytes 8388608 | tf_op jit(solution)/shard_map/all_to_all | solution.py:15
  79.7 0.0 all-gather.5.cloned.1.call-done
  79.7 39.7 %all-gather.7.cloned.1.call-done = bf16[4096,512]{1,0:T(8,128)(2,1)} async-done(((bf16[1024,512]{1,0:T(8,128)(2,1)}), bf16[4096,512]{1,0:T(8,128)(2,1)}) %all-gather.7.cloned.1.call-update) | async-done | bytes 4194320 | tf_op jit(solution)/shard_map/all_gather | solution.py:62
  119.4 7.8 %fusion = bf16[48,32,8,128]{3,2,1,0:T(8,128)(2,1)S(1)} fusion(bf16[512,4096]{0,1:T(8,128)(2,1)} %bitcast.26, bf16[384,4096]{1,0:T(8,128)(2,1)} %all-gather.5.cloned.1.call-done, bf16[4096,512]{1,0:T(8,128)(2,1)} %all-gather.7.cloned.1.call-done), kind=kOutput, calls=%fused_computation.6 | convolution fusion | flops 3223388160 | bytes 14680064 | tf_op jit(solution)/shard_map/dot_general | solution.py:65
  127.2 2.6 copy.37
  129.8 0.0 copy-start
  129.8 0.0 copy-start.1
  129.8 0.0 copy-start.2
  129.8 10.0 %all-to-all-start.1 = ((bf16[32,384,128]{2,1,0:T(8,128)(2,1)}), bf16[32,384,128]{2,1,0:T(8,128)(2,1)S(1)}, u32[]{:S(2)}, u32[]{:S(2)}) async-start(bf16[32,384,128]{2,1,0:T(8,128)(2,1)} %bitcast.24), calls=%async_computation.1 | async-start | bytes 6291456 | tf_op jit(solution)/shard_map/all_to_all | solution.py:34
  139.8 0.0 all-gather.11.cloned.1.call-start
  139.8 0.7 all-gather.11.cloned.1.call-update
  140.5 0.0 all-gather.9.cloned.1.call-start
  140.6 71.3 %all-to-all-done.1 = bf16[32,384,128]{2,1,0:T(8,128)(2,1)S(1)} async-done(((bf16[32,384,128]{2,1,0:T(8,128)(2,1)}), bf16[32,384,128]{2,1,0:T(8,128)(2,1)S(1)}, u32[]{:S(2)}, u32[]{:S(2)}) %all-to-all-start.1) | async-done | bytes 3145760 | tf_op jit(solution)/shard_map/all_to_all | solution.py:34
  211.9 0.4 convert_reduce_fusion.1
  212.3 0.0 copy-done
  212.3 0.2 fusion.8
  212.5 0.1 broadcast_in_dim.4
  212.6 16.4 %all_to_all.41 = f32[32,1,768]{2,1,0:T(1,128)S(1)} all-to-all(f32[32,1,768]{2,1,0:T(1,128)S(1)} %broadcast_in_dim.4), channel_id=1, replica_groups=mesh['ra_0'=8,'ra_1'=4,'cb'=4,'dp'=2] {'ra_0','ra_1'}, dimensions={0} | all-to-all | bytes 196608 | tf_op jit(solution)/shard_map/all_to_all | solution.py:40
  228.9 0.1 reduce_sum.75
  229.0 0.0 copy-done.1
  229.0 0.0 copy-done.2
  229.1 0.2 add_convert_fusion.1
  229.2 12.7 %all_gather.21 = bf16[384,512]{1,0:T(8,128)(2,1)} all-gather(bf16[384,128]{1,0:T(8,128)(2,1)S(1)} %add_convert_fusion.1), channel_id=1, replica_groups=mesh['ra_0'=8,'ra_1'=4,'cb'=4,'dp'=2] {'ra_1'}, dimensions={1}, use_global_device_ids=true | all-gather | bytes 491520 | tf_op jit(solution)/shard_map/all_gather | solution.py:22
  241.9 0.0 all-gather.9.cloned.1.call-update
  241.9 1.7 tile.5
  243.7 47.6 %all_to_all.42 = bf16[512,4,1024]{2,0,1:T(8,128)(2,1)} all-to-all(bf16[512,4,1024]{2,0,1:T(8,128)(2,1)S(1)} %tile.5), channel_id=1, replica_groups=mesh['ra_0'=8,'ra_1'=4,'cb'=4,'dp'=2] {'cb'}, dimensions={1} | all-to-all | bytes 8388608 | tf_op jit(solution)/shard_map/all_to_all | solution.py:15
  291.3 6.2 %copy.23 = bf16[512,4,1024]{0,2,1:T(8,128)(2,1)} copy(bf16[512,4,1024]{2,0,1:T(8,128)(2,1)} %all_to_all.42) | data formatting | bytes 8388608 | tf_op jit(solution)/shard_map/all_to_all | solution.py:15
  297.5 0.0 all-gather.11.cloned.1.call-done
  297.5 7.8 %fusion.1 = bf16[48,32,8,128]{3,2,1,0:T(8,128)(2,1)S(1)} fusion(bf16[512,4096]{0,1:T(8,128)(2,1)} %bitcast.27, bf16[384,4096]{1,0:T(8,128)(2,1)} %all-gather.9.cloned.1.call-done, bf16[4096,512]{1,0:T(8,128)(2,1)} %all-gather.11.cloned.1.call-done), kind=kOutput, calls=%fused_computation.7 | convolution fusion | flops 3223388160 | bytes 14680064 | tf_op jit(solution)/shard_map/dot_general | solution.py:65
  305.3 0.9 copy.36
  306.2 0.0 copy-start.3
  306.2 0.0 copy-start.4
  306.2 74.9 %all_to_all.43 = bf16[32,384,128]{2,1,0:T(8,128)(2,1)S(1)} all-to-all(bf16[32,384,128]{2,1,0:T(8,128)(2,1)S(1)} %bitcast.25), channel_id=1, replica_groups=mesh['ra_0'=8,'ra_1'=4,'cb'=4,'dp'=2] {'ra_0','ra_1'}, dimensions={0} | all-to-all | bytes 6291456 | tf_op jit(solution)/shard_map/all_to_all | solution.py:34
  381.2 0.4 convert_reduce_fusion
  381.6 0.2 fusion.9
  381.8 0.1 broadcast_in_dim.5
  381.8 15.5 %all_to_all.44 = f32[32,1,768]{2,1,0:T(1,128)S(1)} all-to-all(f32[32,1,768]{2,1,0:T(1,128)S(1)} %broadcast_in_dim.5), channel_id=1, replica_groups=mesh['ra_0'=8,'ra_1'=4,'cb'=4,'dp'=2] {'ra_0','ra_1'}, dimensions={0} | all-to-all | bytes 196608 | tf_op jit(solution)/shard_map/all_to_all | solution.py:40
  397.4 0.1 reduce_sum.79
  397.5 0.0 copy-done.3
  397.5 0.0 copy-done.4
  397.5 0.8 add_convert_fusion
  (5 shorter events, 0.0 us)
Async XLA Ops:
  6.5 73.2 %all-gather.5.cloned.1.call-start = ((), (), s32[]{:S(2)}) async-start(), calls=%async_computation.6 | async-start | bytes 3538944 | tf_op jit(solution)/shard_map/all_gather | solution.py:22
  20.4 99.0 %all-gather.7.cloned.1.call-start = ((), (), s32[]{:S(2)}) async-start(), calls=%async_computation.7 | async-start | bytes 5242880 | tf_op jit(solution)/shard_map/all_gather | solution.py:62
  129.8 82.5 %copy-start = (bf16[384,128]{1,0:T(8,128)(2,1)S(1)}, bf16[384,128]{1,0:T(8,128)(2,1)}, u32[]{:S(2)}) copy-start(bf16[384,128]{1,0:T(8,128)(2,1)} %param.9) | copy-start | bytes 294916
  129.8 99.3 %copy-start.1 = (f32[128]{0:T(128)S(1)}, f32[128]{0:T(128)}, u32[]{:S(2)}) copy-start(f32[128]{0:T(128)} %param.15) | copy-start | bytes 1540
  129.8 99.3 %copy-start.2 = (f32[128]{0:T(128)S(1)}, f32[128]{0:T(128)}, u32[]{:S(2)}) copy-start(f32[128]{0:T(128)} %param.14) | copy-start | bytes 1540
  129.8 82.1 %all-to-all-start.1 = ((bf16[32,384,128]{2,1,0:T(8,128)(2,1)}), bf16[32,384,128]{2,1,0:T(8,128)(2,1)S(1)}, u32[]{:S(2)}, u32[]{:S(2)}) async-start(bf16[32,384,128]{2,1,0:T(8,128)(2,1)} %bitcast.24), calls=%async_computation.1 | async-start | bytes 6291456 | tf_op jit(solution)/shard_map/all_to_all | solution.py:34
  139.8 157.7 %all-gather.11.cloned.1.call-start = ((), (), s32[]{:S(2)}) async-start(), calls=%async_computation.9 | async-start | bytes 5242880 | tf_op jit(solution)/shard_map/all_gather | solution.py:62
  140.5 157.0 %all-gather.9.cloned.1.call-start = ((), (), s32[]{:S(2)}) async-start(), calls=%async_computation.8 | async-start | bytes 3538944 | tf_op jit(solution)/shard_map/all_gather | solution.py:22
  306.2 91.3 %copy-start.3 = (f32[128]{0:T(128)S(1)}, f32[128]{0:T(128)}, u32[]{:S(2)}) copy-start(f32[128]{0:T(128)} %param.17) | copy-start | bytes 1540
  306.2 91.3 %copy-start.4 = (f32[128]{0:T(128)S(1)}, f32[128]{0:T(128)}, u32[]{:S(2)}) copy-start(f32[128]{0:T(128)} %param.16) | copy-start | bytes 1540
Sparse Core Ops, SparseCore 0:
  20.5 48.2 all-gather.4
  70.6 48.7 all-gather.6
  142.4 51.0 all-gather.10
  242.1 40.5 all-gather.8
